TPU v7x, 32 devices: a whole 2x2x4 slice. The times are simulated.
32 devices in a mesh: fs: 16 (over z, y, x), tp: 2 (over core).
Axes of the slice: x: 2, y: 2, z: 4, core: 2. Of those that a mesh axis runs over, the one named last changes fastest.
Arguments:
- tokens: bfloat16 [6144, 2048], P('fs'), may hold values from -6 to 6
- merged: bfloat16 [6144, 2048], P('fs'), may hold values from -6 to 6
- gain_first: float32 [2048], replicated, may hold values from 0.1 to 1.9
- gate_first: bfloat16 [2048, 2816], P('fs', 'tp'), may hold values from -0.125 to 0.125
- up_first: bfloat16 [2048, 2816], P('fs', 'tp'), may hold values from -0.125 to 0.125
- down_first: bfloat16 [2816, 2048], P('tp', 'fs'), may hold values from -0.21875 to 0.21875
- gain_second: float32 [2048], replicated, may hold values from 0.1 to 1.9
- gate_second: bfloat16 [2048, 2816], P('fs', 'tp'), may hold values from -0.125 to 0.125
- up_second: bfloat16 [2048, 2816], P('fs', 'tp'), may hold values from -0.125 to 0.125
- down_second: bfloat16 [2816, 2048], P('tp', 'fs'), may hold values from -0.21875 to 0.21875
Outputs:
- result: bfloat16 [6144, 2048], P('fs')
All inputs are finite; a program needn't handle non-finite values.
Results may differ from a plain program's by a relative error of at most 0.01.
Values may be sent and summed in bfloat16 or wider, within the bound.
A program may use at most 64 MiB of HBM per device.

v0:
```python
import jax
import jax.numpy as jnp
from jax import lax
from jax.sharding import PartitionSpec as P

EPS = 1e-06


def norm_rows(values, gain):
    scale = lax.rsqrt(jnp.mean(values * values, axis=-1, keepdims=True) + EPS)
    return values * scale * gain


def make_folder(normed, pieces):
    return (
        jnp.dot(normed, pieces[0], preferred_element_type=jnp.float32),
        jnp.dot(normed, pieces[1], preferred_element_type=jnp.float32),
    )


def shards(
    tokens,
    merged,
    gain_first,
    gate_first,
    up_first,
    down_first,
    gain_second,
    gate_second,
    up_second,
    down_second,
):
    normed_first = norm_rows(tokens.astype(jnp.float32), gain_first).astype(jnp.bfloat16)
    gate, up = make_folder(
        normed_first,
        (
            lax.all_gather(gate_first, "fs", axis=0, tiled=True),
            lax.all_gather(up_first, "fs", axis=0, tiled=True),
        ),
    )
    hidden = (jax.nn.silu(gate) * up).astype(jnp.bfloat16)
    down_whole = lax.all_gather(down_first, "fs", axis=1, tiled=True)
    partial_value = jnp.dot(hidden, down_whole, preferred_element_type=jnp.float32)
    first_sum = lax.psum(partial_value.astype(jnp.bfloat16), "tp").astype(jnp.float32)
    middle = tokens.astype(jnp.float32) + merged.astype(jnp.float32) + 0.5 * first_sum
    normed_second = norm_rows(middle, gain_second).astype(jnp.bfloat16)
    gate_two, up_two = make_folder(
        normed_second,
        (
            lax.all_gather(gate_second, "fs", axis=0, tiled=True),
            lax.all_gather(up_second, "fs", axis=0, tiled=True),
        ),
    )
    hidden_two = (jax.nn.silu(gate_two) * up_two).astype(jnp.bfloat16)
    down_two = lax.all_gather(down_second, "fs", axis=1, tiled=True)
    partial_two = jnp.dot(hidden_two, down_two, preferred_element_type=jnp.float32)
    second_sum = lax.psum(partial_two.astype(jnp.bfloat16), "tp").astype(jnp.float32)
    return (middle + 0.5 * second_sum).astype(jnp.bfloat16)


def solution(mesh):
    return jax.shard_map(
        shards,
        mesh=mesh,
        in_specs=(
            P("fs", None),
            P("fs", None),
            P(),
            P("fs", "tp"),
            P("fs", "tp"),
            P("tp", "fs"),
            P(),
            P("fs", "tp"),
            P("fs", "tp"),
            P("tp", "fs"),
        ),
        out_specs=P("fs", None),
        check_vma=False,
    )
```

profile of v0, /device:TPU:0, one launch (start us, length us, event | category | flops | bytes accessed | tf_op | source)
XLA Modules:
  0.0 665.2 jit_solution(4083028435205835512)
XLA Ops:
  6.5 0.7 all-gather.7.cloned.1.call-update
  7.3 0.0 all-gather.11.cloned.1.call-start
  7.3 0.7 all-gather.11.cloned.1.call-update
  8.0 0.0 all-gather.9.cloned.1.call-start
  8.1 0.7 all-gather.9.cloned.1.call-update
  8.7 0.0 all-reduce.3.cloned.1.call-start
  8.8 1.8 fusion.1
  10.6 0.0 copy-start.4
  10.6 90.9 %all-gather.7.cloned.1.call-done = bf16[2048,1408]{1,0:T(8,128)(2,1)} async-done(((bf16[128,1408]{1,0:T(8,128)(2,1)}), bf16[2048,1408]{1,0:T(8,128)(2,1)}) %all-gather.7.cloned.1.call-update) | async-done | bytes 5767184 | tf_op jit(solution)/shard_map/all_gather | solution.py:37
  101.5 7.1 %fusion.8 = f32[384,1408]{1,0:T(8,128)} fusion(bf16[2048,1408]{1,0:T(8,128)(2,1)} %all-gather.7.cloned.1.call-done, bf16[384,2048]{1,0:T(8,128)(2,1)} %param.10, f32[2048]{0:T(1024)} %param.12, f32[384]{0:T(512)S(1)} %add_rsqrt_fusion.1), kind=kOutput, calls=%fused_computation.16 | convolution fusion | flops 2217738240 | bytes 9512448 | tf_op jit(solution)/shard_map/dot_general | solution.py:16
  108.7 102.6 %all-gather.11.cloned.1.call-done = bf16[1408,2048]{1,0:T(8,128)(2,1)} async-done(((bf16[1408,128]{1,0:T(8,128)(2,1)}), bf16[1408,2048]{1,0:T(8,128)(2,1)}) %all-gather.11.cloned.1.call-update) | async-done | bytes 5767184 | tf_op jit(solution)/shard_map/all_gather | solution.py:42
  211.3 89.7 %all-gather.9.cloned.1.call-done = bf16[2048,1408]{1,0:T(8,128)(2,1)} async-done(((bf16[128,1408]{1,0:T(8,128)(2,1)}), bf16[2048,1408]{1,0:T(8,128)(2,1)}) %all-gather.9.cloned.1.call-update) | async-done | bytes 5767184 | tf_op jit(solution)/shard_map/all_gather | solution.py:38
  300.9 11.2 %convolution_convert_fusion.1 = bf16[384,2048]{1,0:T(8,128)(2,1)} fusion(bf16[1408,2048]{1,0:T(8,128)(2,1)} %all-gather.11.cloned.1.call-done, bf16[2048,1408]{1,0:T(8,128)(2,1)} %all-gather.9.cloned.1.call-done, f32[384,1408]{1,0:T(8,128)} %fusion.8, bf16[384,2048]{1,0:T(8,128)(2,1)S(1)} %copy-done, f32[2048]{0:T(1024)S(1)} %copy-done.4, ...), kind=kOutput, calls=%fused_computation.15 | convolution fusion | flops 4436361216 | bytes 16852480 | tf_op jit(solution)/shard_map/dot_general | solution.py:43
  312.1 0.0 all-reduce.3.cloned.1.call-update
  312.2 0.0 all-gather.13.cloned.1.call-start
  312.2 0.5 all-gather.13.cloned.1.call-update
  312.8 0.0 all-gather.15.cloned.1.call-start
  312.8 0.5 all-gather.15.cloned.1.call-update
  313.3 0.0 all-gather.17.cloned.1.call-start
  313.4 0.7 all-gather.17.cloned.1.call-update
  314.1 0.2 all-reduce.5.cloned.1.call-start
  314.3 17.0 %all-reduce.3.cloned.1.call-done = bf16[384,2048]{1,0:T(8,128)(2,1)} async-done(((bf16[384,2048]{1,0:T(8,128)(2,1)}), bf16[384,2048]{1,0:T(8,128)(2,1)}) %all-reduce.3.cloned.1.call-update) | async-done | bytes 1572880 | tf_op jit(solution)/shard_map/psum | solution.py:44
  331.3 2.4 multiply_reduce_fusion
  333.8 2.2 multiply_convert_fusion
  336.0 87.8 %all-gather.13.cloned.1.call-done = bf16[2048,1408]{1,0:T(8,128)(2,1)} async-done(((bf16[128,1408]{1,0:T(8,128)(2,1)}), bf16[2048,1408]{1,0:T(8,128)(2,1)}) %all-gather.13.cloned.1.call-update) | async-done | bytes 5767184 | tf_op jit(solution)/shard_map/all_gather | solution.py:50
  423.8 7.1 %fusion.12 = f32[384,1408]{1,0:T(8,128)} fusion(bf16[384,2048]{1,0:T(8,128)(2,1)} %multiply_convert_fusion, bf16[2048,1408]{1,0:T(8,128)(2,1)} %all-gather.13.cloned.1.call-done), kind=kOutput, calls=%fused_computation.21 | convolution fusion | flops 2214592512 | bytes 9502720 | tf_op jit(solution)/shard_map/dot_general | solution.py:16
  430.9 82.9 %all-gather.15.cloned.1.call-done = bf16[2048,1408]{1,0:T(8,128)(2,1)} async-done(((bf16[128,1408]{1,0:T(8,128)(2,1)}), bf16[2048,1408]{1,0:T(8,128)(2,1)}) %all-gather.15.cloned.1.call-update) | async-done | bytes 5767184 | tf_op jit(solution)/shard_map/all_gather | solution.py:51
  513.8 109.7 %all-gather.17.cloned.1.call-done = bf16[1408,2048]{1,0:T(8,128)(2,1)} async-done(((bf16[1408,128]{1,0:T(8,128)(2,1)}), bf16[1408,2048]{1,0:T(8,128)(2,1)}) %all-gather.17.cloned.1.call-update) | async-done | bytes 5767184 | tf_op jit(solution)/shard_map/all_gather | solution.py:55
  623.6 11.7 %convolution_convert_fusion = bf16[384,2048]{1,0:T(8,128)(2,1)} fusion(bf16[1408,2048]{1,0:T(8,128)(2,1)} %all-gather.17.cloned.1.call-done, bf16[384,2048]{1,0:T(8,128)(2,1)} %multiply_convert_fusion, bf16[2048,1408]{1,0:T(8,128)(2,1)} %all-gather.15.cloned.1.call-done, f32[384,1408]{1,0:T(8,128)} %fusion.12), kind=kOutput, calls=%fused_computation.14 | convolution fusion | flops 4433215488 | bytes 16842752 | tf_op jit(solution)/shard_map/dot_general | solution.py:56
  635.3 0.0 all-reduce.5.cloned.1.call-update
  635.3 18.7 %all-reduce.5.cloned.1.call-done = bf16[384,2048]{1,0:T(8,128)(2,1)} async-done(((bf16[384,2048]{1,0:T(8,128)(2,1)}), bf16[384,2048]{1,0:T(8,128)(2,1)}) %all-reduce.5.cloned.1.call-update) | async-done | bytes 1572880 | tf_op jit(solution)/shard_map/psum | solution.py:57
  654.0 4.3 add_convert_fusion
  (12 shorter events, 0.0 us)
Async XLA Ops:
  6.5 95.0 %all-gather.7.cloned.1.call-start = ((), (), s32[]{:S(2)}) async-start(), calls=%async_computation | async-start | bytes 6127616 | tf_op jit(solution)/shard_map/all_gather | solution.py:37
  7.3 204.0 %all-gather.11.cloned.1.call-start = ((), (), s32[]{:S(2)}) async-start(), calls=%async_computation.2 | async-start | bytes 6127616 | tf_op jit(solution)/shard_map/all_gather | solution.py:42
  8.0 292.9 %all-gather.9.cloned.1.call-start = ((), (), s32[]{:S(2)}) async-start(), calls=%async_computation.1 | async-start | bytes 6127616 | tf_op jit(solution)/shard_map/all_gather | solution.py:38
  8.7 322.6 %all-reduce.3.cloned.1.call-start = ((), (), s32[]{:S(2)}) async-start(), calls=%async_computation.3 | async-start | bytes 3145728 | tf_op jit(solution)/shard_map/psum | solution.py:44
  10.6 290.3 %copy-start = (bf16[384,2048]{1,0:T(8,128)(2,1)S(1)}, bf16[384,2048]{1,0:T(8,128)(2,1)}, u32[]{:S(2)}) copy-start(bf16[384,2048]{1,0:T(8,128)(2,1)} %param.10) | copy-start | bytes 4718596
  10.6 290.3 %copy-start.4 = (f32[2048]{0:T(1024)S(1)}, f32[2048]{0:T(1024)}, u32[]{:S(2)}) copy-start(f32[2048]{0:T(1024)} %param.12) | copy-start | bytes 24580
  312.1 19.2 %copy-start.1 = (bf16[384,2048]{1,0:T(8,128)(2,1)S(1)}, bf16[384,2048]{1,0:T(8,128)(2,1)}, u32[]{:S(2)}) copy-start(bf16[384,2048]{1,0:T(8,128)(2,1)} %param.11) | copy-start | bytes 4718596
  312.2 21.6 %copy-start.3 = (f32[2048]{0:T(1024)S(1)}, f32[2048]{0:T(1024)}, u32[]{:S(2)}) copy-start(f32[2048]{0:T(1024)} %param.16) | copy-start | bytes 24580
  312.2 111.7 %all-gather.13.cloned.1.call-start = ((), (), s32[]{:S(2)}) async-start(), calls=%async_computation.4 | async-start | bytes 6127616 | tf_op jit(solution)/shard_map/all_gather | solution.py:50
  312.8 201.1 %all-gather.15.cloned.1.call-start = ((), (), s32[]{:S(2)}) async-start(), calls=%async_computation.5 | async-start | bytes 6127616 | tf_op jit(solution)/shard_map/all_gather | solution.py:51
  313.3 310.2 %all-gather.17.cloned.1.call-start = ((), (), s32[]{:S(2)}) async-start(), calls=%async_computation.6 | async-start | bytes 6127616 | tf_op jit(solution)/shard_map/all_gather | solution.py:55
  314.1 340.0 %all-reduce.5.cloned.1.call-start = ((), (), s32[]{:S(2)}) async-start(), calls=%async_computation.7 | async-start | bytes 3145728 | tf_op jit(solution)/shard_map/psum | solution.py:57
  331.3 2.4 copy-start.2
Sparse Core Ops, SparseCore 0:
  10.0 91.4 all-gather.6
  104.2 106.9 all-gather.10
  213.9 86.9 all-gather.8
  312.3 19.0 all-reduce.2
  333.9 89.9 all-gather.12
  426.4 87.4 all-gather.14
  516.5 106.9 all-gather.16
  635.4 18.5 all-reduce.4
where the time goes:
time: 665 us
  waiting for transfers between devices  603 us (91%)
  matrix products  37.1 us (6%)
  between operations  13.5 us (2%)
  other arithmetic  10.8 us (2%)
    all_gather x1, waiting for transfers between devices, shards(): down_two = lax.all_gather(down_second, 'fs', axis=1, tiled=True)  110 us
    all_gather x1, waiting for transfers between devices, shards(): down_whole = lax.all_gather(down_first, 'fs', axis=1, tiled=True)  103 us
    all_gather x1, waiting for transfers between devices, shards(): lax.all_gather(gate_first, 'fs', axis=0, tiled=True)  90.9 us
    all_gather x1, waiting for transfers between devices, shards(): lax.all_gather(up_first, 'fs', axis=0, tiled=True)  89.7 us
    all_gather x1, waiting for transfers between devices, shards(): lax.all_gather(gate_second, 'fs', axis=0, tiled=True)  87.8 us
    all_gather x1, waiting for transfers between devices, shards(): lax.all_gather(up_second, 'fs', axis=0, tiled=True)  82.9 us
    psum x1, waiting for transfers between devices, shards(): lax.psum(partial_two.astype(jnp.bfloat16), 'tp').astype(jnp.float32)  18.7 us
    psum x1, waiting for transfers between devices, shards(): lax.psum(partial_value.astype(jnp.bfloat16), 'tp').astype(jnp.float32)  17 us
  transfers between devices with their start and end apart: 8, of which 8 were waited for; matrix products, arithmetic and copies ran while one was open for 3% of the time, Pallas kernels for 0%

commit v1 on v0

v1 whole, which is shorter than its diff:
```python
import functools

import jax
import jax.numpy as jnp
from jax import lax
from jax.experimental import pallas as pl
from jax.experimental.pallas import tpu as pltpu
from jax.sharding import PartitionSpec as P

EPS = 1e-06
BF16 = jnp.bfloat16
F32 = jnp.float32
PLANE = 4
RING = 4


def norm_rows(values, gain):
    scale = lax.rsqrt(jnp.mean(values * values, axis=-1, keepdims=True) + EPS)
    return values * scale * gain


def gathered_block(normed, gate, up, down):
    gate_whole = lax.all_gather(gate, "fs", axis=0, tiled=True)
    up_whole = lax.all_gather(up, "fs", axis=0, tiled=True)
    g = jnp.dot(normed, gate_whole, preferred_element_type=F32)
    u = jnp.dot(normed, up_whole, preferred_element_type=F32)
    hidden = (jax.nn.silu(g) * u).astype(BF16)
    down_whole = lax.all_gather(down, "fs", axis=1, tiled=True)
    part = jnp.dot(hidden, down_whole, preferred_element_type=F32)
    return lax.psum(part.astype(BF16), "tp").astype(F32)


def gathered_shards(tokens, merged, gain1, g1, u1, d1, gain2, g2, u2, d2):
    source = tokens.astype(F32)
    middle = source + merged.astype(F32)
    normed = norm_rows(source, gain1).astype(BF16)
    middle = middle + 0.5 * gathered_block(normed, g1, u1, d1)
    normed = norm_rows(middle, gain2).astype(BF16)
    return (middle + 0.5 * gathered_block(normed, g2, u2, d2)).astype(BF16)


def kernel(
    tokens, merged, gain1, gain2, wa, wb, wc, wd, we, wf, out,
    w, normed1, normed2, hidden, part, own, sib, comb, rsr, middle, fin,
    p1_s, p1_r, p1_l, ring_s, ring_r, fwd_s, fwd_r,
    ag_s, ag_r, rel_s, rel_r, sib_s, sib_r, rs_s, rs_r, fin_s, fin_r,
):
    shards_in = (wa, wb, wc, wd, we, wf)
    fs = lax.axis_index("fs")
    t = lax.axis_index("tp")
    z = fs // PLANE
    p = fs % PLANE
    rows, width = tokens.shape
    half = rows // 2
    q, pw = w.shape[1], width // RING
    ds = wa.shape[1]
    qh = q // 2

    def dev(zz, pp, tt):
        return {"fs": zz * PLANE + pp, "tp": tt}

    def plane_peer(r):
        return (p + r) % PLANE

    zc, zb, zo = (z + 1) % RING, (z + RING - 1) % RING, (z + 2) % RING
    cw, ccw, sibling = dev(zc, p, t), dev(zb, p, t), dev(z, p, 1 - t)

    def remote(src, dst, s, r, to):
        return pltpu.make_async_remote_copy(
            src_ref=src, dst_ref=dst, send_sem=s, recv_sem=r,
            device_id=to, device_id_type=pl.DeviceIdType.MESH,
        )

    mine = pl.ds(pl.multiple_of(t * half, 16), half)
    other = pl.ds(pl.multiple_of((1 - t) * half, 16), half)

    barrier = pltpu.get_barrier_semaphore()
    targets = [cw, ccw, sibling] + [dev(z, plane_peer(r), t) for r in (1, 2, 3)]
    for to in targets:
        pl.semaphore_signal(barrier, inc=1, device_id=to, device_id_type=pl.DeviceIdType.MESH)
    pl.semaphore_wait(barrier, len(targets))

    def p1_lanes(pp):
        return pl.ds(pl.multiple_of((z * PLANE + pp) * ds, ds), ds)

    def p1(m, r):
        peer = plane_peer(r)
        src = shards_in[m].at[pl.ds(pl.multiple_of(peer * q, 16), q), :]
        return remote(src, w.at[m, :, p1_lanes(p)], p1_s.at[m, r - 1], p1_r.at[m, r - 1], dev(z, peer, t))

    def p1_local(m):
        src = shards_in[m].at[pl.ds(pl.multiple_of(p * q, 16), q), :]
        return pltpu.make_async_copy(src, w.at[m, :, p1_lanes(p)], p1_l.at[m])

    def p1_in(m, r):
        src = w.at[m, :, p1_lanes((p + PLANE - r) % PLANE)]
        return remote(src, src, p1_s.at[m, r - 1], p1_r.at[m, r - 1], dev(z, plane_peer(r), t))

    def start_p1(m):
        for r in (1, 2, 3):
            p1(m, r).start()
        p1_local(m).start()

    def blk(m, zz, lo=0, n=None):
        return w.at[m, pl.ds(lo, q if n is None else n), pl.ds(pl.multiple_of(zz * pw, pw), pw)]

    def ring(m, k, zz):
        return remote(blk(m, zz), blk(m, zz), ring_s.at[m, k], ring_r.at[m, k], (cw, ccw)[k])

    def fwd(m, k, zz):
        return remote(blk(m, zz, k * qh, qh), blk(m, zz, k * qh, qh), fwd_s.at[m, k], fwd_r.at[m, k], (cw, ccw)[k])

    def own_ring(m):
        p1_local(m).wait()
        for r in (1, 2, 3):
            p1_in(m, r).wait_recv()
        ring(m, 0, z).start()
        ring(m, 1, z).start()

    def service(m):
        ring(m, 0, zb).wait_recv()
        fwd(m, 0, zb).start()
        ring(m, 1, zc).wait_recv()
        fwd(m, 1, zc).start()

    def arrived(m):
        fwd(m, 0, zo).wait_recv()
        fwd(m, 1, zo).wait_recv()

    def ag(f, r, slot):
        buf = (normed1, normed2)[f]
        return remote(buf.at[slot, mine, :], buf.at[r, mine, :], ag_s.at[f, r - 1], ag_r.at[f, r - 1], dev(z, plane_peer(r), t))

    def relay(f, r, which):
        buf = (normed1, normed2)[f]
        return remote(buf.at[r, which, :], buf.at[r, which, :], rel_s.at[f, r], rel_r.at[f, r], sibling)

    def ag_start(f):
        for r in (3, 1, 2):
            ag(f, r, 0).start()

    def ag_relay(f):
        for r in (1, 2, 3):
            ag(f, r, r).wait_recv()
            relay(f, r, mine).start()

    def to_sibling(f, r):
        return remote(part.at[r], sib.at[r], sib_s.at[f, r], sib_r.at[f, r], sibling)

    def rs(f, r):
        return remote(comb.at[r - 1], rsr.at[r - 1], rs_s.at[f, r - 1], rs_r.at[f, r - 1], dev(z, (p + PLANE - r) % PLANE, t))

    def make_hidden(f, slot):
        buf = (normed1, normed2)[f]

        @pl.loop(0, 2)
        def _(i):
            at = pl.ds(pl.multiple_of(i * half, 16), half)
            x = buf[slot, at, :]
            dims = (((1,), (1,)), ((), ()))
            g = lax.dot_general(x, w[3 * f], dims, preferred_element_type=F32)
            u = lax.dot_general(x, w[3 * f + 1], dims, preferred_element_type=F32)
            hidden[slot, at, :] = (g / (1.0 + jnp.exp(-g)) * u).astype(BF16)

    def make_down(f, r):
        @pl.loop(0, RING)
        def _(c):
            at = pl.ds(pl.multiple_of(c * pw, pw), pw)
            part[r, :, at] = jnp.dot(hidden[r, other, :], w[3 * f + 2, :, at], preferred_element_type=F32).astype(BF16)

        to_sibling(f, r).start()

        @pl.loop(0, RING)
        def _(c):
            at = pl.ds(pl.multiple_of(c * pw, pw), pw)
            own[r, :, at] = jnp.dot(hidden[r, mine, :], w[3 * f + 2, :, at], preferred_element_type=F32).astype(BF16)

    step = 16

    def combine(f, r):
        to_sibling(f, r).wait_recv()

        @pl.loop(0, half // step)
        def _(i):
            at = pl.ds(pl.multiple_of(i * step, step), step)
            comb[r - 1, at, :] = (own[r, at, :].astype(F32) + sib[r, at, :].astype(F32)).astype(BF16)

        rs(f, r).start()

    def all_down(f):
        order = (3, 1, 2, 0)
        for k, r in enumerate(order):
            make_down(f, r)
            if k:
                combine(f, order[k - 1])
        to_sibling(f, 0).wait_recv()

    def reduced(at):
        total = own[0, at, :].astype(F32) + sib[0, at, :].astype(F32)
        for r in (1, 2, 3):
            total = total + rsr[r - 1, at, :].astype(F32)
        return total

    start_p1(0)
    start_p1(1)
    start_p1(2)

    @pl.loop(0, rows // step)
    def _(i):
        at = pl.ds(pl.multiple_of(i * step, step), step)
        normed1[0, at, :] = norm_rows(tokens[at, :].astype(F32), gain1[...]).astype(BF16)

    ag_start(0)
    for m in (3, 4, 5):
        start_p1(m)
    own_ring(0)
    own_ring(1)
    service(0)
    own_ring(2)
    ag_relay(0)
    service(1)
    own_ring(3)
    arrived(0)
    arrived(1)
    make_hidden(0, 0)
    for r in (1, 2, 3):
        relay(0, r, other).wait_recv()
        make_hidden(0, r)
    service(2)
    own_ring(4)
    arrived(2)
    all_down(0)
    service(3)
    own_ring(5)
    service(4)
    for r in (1, 2, 3):
        rs(0, r).wait_recv()

    @pl.loop(0, half // step)
    def _(i):
        at = pl.ds(pl.multiple_of(i * step, step), step)
        full = pl.ds(pl.multiple_of(t * half + i * step, step), step)
        value = tokens[full, :].astype(F32) + merged[full, :].astype(F32) + 0.5 * reduced(at)
        middle[at, :] = value
        normed2[0, full, :] = norm_rows(value, gain2[...]).astype(BF16)

    ag_start(1)
    relay(1, 0, mine).start()
    service(5)
    arrived(3)
    arrived(4)
    relay(1, 0, other).wait_recv()
    make_hidden(1, 0)
    ag_relay(1)
    for r in (1, 2, 3):
        relay(1, r, other).wait_recv()
        make_hidden(1, r)
    for r in range(PLANE):
        to_sibling(0, r).wait_send()
    for r in (1, 2, 3):
        rs(0, r).wait_send()
    arrived(5)
    all_down(1)
    for r in (1, 2, 3):
        rs(1, r).wait_recv()

    @pl.loop(0, half // step)
    def _(i):
        at = pl.ds(pl.multiple_of(i * step, step), step)
        full = pl.ds(pl.multiple_of(t * half + i * step, step), step)
        out[full, :] = (middle[at, :] + 0.5 * reduced(at)).astype(BF16)

    last = remote(out.at[mine, :], fin, fin_s, fin_r, sibling)
    last.start()
    for m in range(6):
        for r in (1, 2, 3):
            p1(m, r).wait_send()
        for k in range(2):
            ring(m, k, z).wait_send()
            fwd(m, k, (zb, zc)[k]).wait_send()
    for f in range(2):
        for r in (1, 2, 3):
            ag(f, r, 0).wait_send()
            relay(f, r, mine).wait_send()
    relay(1, 0, mine).wait_send()
    for r in range(PLANE):
        to_sibling(1, r).wait_send()
    for r in (1, 2, 3):
        rs(1, r).wait_send()
    last.wait_recv()
    out[other, :] = fin[...]
    last.wait_send()


def plane_shards(tokens, merged, gain1, g1, u1, d1, gain2, g2, u2, d2):
    rows, width = tokens.shape
    half = rows // 2
    q = d1.shape[0] // PLANE
    vmem = pl.BlockSpec(memory_space=pltpu.VMEM)
    dma = lambda *s: pltpu.SemaphoreType.DMA(s)
    return pl.pallas_call(
        kernel,
        out_shape=jax.ShapeDtypeStruct((rows, width), BF16),
        in_specs=[vmem] * 10,
        out_specs=vmem,
        scratch_shapes=[
            pltpu.VMEM((6, q, width), BF16),
            pltpu.VMEM((PLANE, rows, width), BF16),
            pltpu.VMEM((PLANE, rows, width), BF16),
            pltpu.VMEM((PLANE, rows, q), BF16),
            pltpu.VMEM((PLANE, half, width), BF16),
            pltpu.VMEM((PLANE, half, width), BF16),
            pltpu.VMEM((PLANE, half, width), BF16),
            pltpu.VMEM((PLANE - 1, half, width), BF16),
            pltpu.VMEM((PLANE - 1, half, width), BF16),
            pltpu.VMEM((half, width), F32),
            pltpu.VMEM((half, width), BF16),
            dma(6, 3), dma(6, 3), dma(6),
            dma(6, 2), dma(6, 2), dma(6, 2), dma(6, 2),
            dma(2, 3), dma(2, 3), dma(2, 4), dma(2, 4),
            dma(2, 4), dma(2, 4), dma(2, 3), dma(2, 3),
            pltpu.SemaphoreType.DMA, pltpu.SemaphoreType.DMA,
        ],
        compiler_params=pltpu.CompilerParams(
            collective_id=0, has_side_effects=True, vmem_limit_bytes=60 * 2**20
        ),
    )(tokens, merged, gain1[None], gain2[None], g1.T, u1.T, d1, g2.T, u2.T, d2)


def shards(n_fs, n_tp, *args):
    rows, width = args[0].shape
    hid, cols = args[5].shape
    fits = n_fs == PLANE * RING and n_tp == 2 and cols % 128 == 0
    fits = fits and hid % (32 * PLANE) == 0 and rows % 32 == 0
    return plane_shards(*args) if fits else gathered_shards(*args)


def solution(mesh):
    return jax.shard_map(
        functools.partial(shards, mesh.shape["fs"], mesh.shape["tp"]),
        mesh=mesh,
        in_specs=(
            P("fs", None),
            P("fs", None),
            P(),
            P("fs", "tp"),
            P("fs", "tp"),
            P("tp", "fs"),
            P(),
            P("fs", "tp"),
            P("fs", "tp"),
            P("tp", "fs"),
        ),
        out_specs=P("fs", None),
        check_vma=False,
    )
```

time: 665 us -> 247 us (0.37)
  waiting for transfers between devices: 603 us -> 0 us
  Pallas kernels: 0 us -> 234 us
  matrix products: 37.1 us -> 0 us
  between operations: 13.5 us -> 0.01 us
  other arithmetic: 10.8 us -> 0 us
  local copies, waits for them, and re-layouts: 0.02 us -> 8.42 us
    all_gather x6 -> x0, waiting for transfers between devices: 564 us -> none  [the longest x1 110 us: shards(): down_two = lax.all_gather(down_second, 'fs', axis=1, tiled=True)]
    pallas_call x0 -> x1, Pallas kernels: none -> 234 us  [plane_shards(): pl.pallas_call(kernel, out_shape=jax.ShapeDtypeStruct((rows, width), BF16...]
    dot_general x4 -> x0, matrix products: 37.1 us -> none  [the longest x2 14.2 us: make_folder(): jnp.dot(normed, pieces[0], preferred_element_type=jnp.float32)]
    psum x2 -> x0, waiting for transfers between devices: 35.7 us -> none  [the longest x1 18.7 us: shards(): lax.psum(partial_two.astype(jnp.bfloat16), 'tp').astype(jnp.float32)]
    unnamed x10 -> x9, local copies, waits for them, and re-layouts: 0.02 us -> 8.42 us
  transfers between devices with their start and end apart: 8 -> 0, of which waited for: 8 -> 0; matrix products, arithmetic and copies ran while one was open for 3% -> 0% of each run, Pallas kernels for 0% -> 0%
where the time goes in v1:
time: 247 us; the launch traced here: 243 us
  Pallas kernels  234 us (95%)
  local copies, waits for them, and re-layouts  8.42 us (3%)
    pallas_call x1, Pallas kernels, plane_shards(): pl.pallas_call(kernel, out_shape=jax.ShapeDtypeStruct((rows, width), BF16...  234 us
    unnamed x9, local copies, waits for them, and re-layouts  8.42 us

profile of v1, /device:TPU:0, one launch (start us, length us, event | category | flops | bytes accessed | tf_op | source)
XLA Modules:
  0.0 242.9 jit_solution(10906744405664986699)
XLA Ops:
  0.0 0.0 copy-start.1
  0.0 0.0 copy-start
  0.0 2.0 copy.11
  2.0 1.9 copy.12
  3.8 0.0 copy-done
  3.9 0.9 copy.13
  4.8 0.0 copy-done.1
  4.8 0.9 copy.14
  5.7 234.5 %shard_map.100 = bf16[384,2048]{1,0:T(8,128)(2,1)} custom-call(bf16[384,2048]{1,0:T(8,128)(2,1)} %tokens.1, bf16[384,2048]{1,0:T(8,128)(2,1)} %merged.1, f32[1,2048]{1,0:T(1,128)} %bitcast.10, f32[1,2048]{1,0:T(1,128)} %bitcast.11, bf16[1408,128]{1,0:T(8,128)(2,1)} %bitcast.6, bf16[1408,128]{1,0:T(8,128)(2,1)} %bitcast.7, bf16[1408,128]{1,0:T(8,128)(2,1)} %wc.1, ...), custom_call_target="tpu_custom_call" | custom-call | tf_op jit(solution)/shard_map/pallas_call | solution.py:301
  240.2 2.7 %copy.16 = bf16[384,2048]{1,0:T(8,128)(2,1)} copy(bf16[384,2048]{1,0:T(8,128)(2,1)} %shard_map.100) | data formatting | bytes 3145728
Async XLA Ops:
  0.0 4.8 %copy-start.1 = (bf16[128,1408]{1,0:T(8,128)(2,1)S(1)}, bf16[128,1408]{1,0:T(8,128)(2,1)}, u32[]{:S(2)}) copy-start(bf16[128,1408]{1,0:T(8,128)(2,1)} %param.18) | copy-start | bytes 1081348
  0.0 3.8 %copy-start = (bf16[128,1408]{1,0:T(8,128)(2,1)S(1)}, bf16[128,1408]{1,0:T(8,128)(2,1)}, u32[]{:S(2)}) copy-start(bf16[128,1408]{1,0:T(8,128)(2,1)} %param.17) | copy-start | bytes 1081348

commit v2 on v1

v2 whole, which is shorter than its diff:
```python
import functools

import jax
import jax.numpy as jnp
from jax import lax
from jax.experimental import pallas as pl
from jax.experimental.pallas import tpu as pltpu
from jax.sharding import PartitionSpec as P

EPS = 1e-06
BF16 = jnp.bfloat16
F32 = jnp.float32
PLANE = 4
RING = 4


def norm_rows(values, gain):
    scale = lax.rsqrt(jnp.mean(values * values, axis=-1, keepdims=True) + EPS)
    return values * scale * gain


def gathered_block(normed, gate, up, down):
    gate_whole = lax.all_gather(gate, "fs", axis=0, tiled=True)
    up_whole = lax.all_gather(up, "fs", axis=0, tiled=True)
    g = jnp.dot(normed, gate_whole, preferred_element_type=F32)
    u = jnp.dot(normed, up_whole, preferred_element_type=F32)
    hidden = (jax.nn.silu(g) * u).astype(BF16)
    down_whole = lax.all_gather(down, "fs", axis=1, tiled=True)
    part = jnp.dot(hidden, down_whole, preferred_element_type=F32)
    return lax.psum(part.astype(BF16), "tp").astype(F32)


def gathered_shards(tokens, merged, gain1, g1, u1, d1, gain2, g2, u2, d2):
    source = tokens.astype(F32)
    middle = source + merged.astype(F32)
    normed = norm_rows(source, gain1).astype(BF16)
    middle = middle + 0.5 * gathered_block(normed, g1, u1, d1)
    normed = norm_rows(middle, gain2).astype(BF16)
    return (middle + 0.5 * gathered_block(normed, g2, u2, d2)).astype(BF16)


def kernel(
    tokens, merged, gain1, gain2, wa, wb, wc, wd, we, wf, out,
    w, normed1, normed2, hidden, part, own, sib, comb, diag, rsr, middle, fin,
    p1_s, p1_r, p1_l, ring_s, ring_r, fwd_s, fwd_r,
    ag_s, ag_r, rel_s, rel_r, sib_s, sib_r, rs_s, rs_r, fin_s, fin_r,
):
    shards_in = (wa, wb, wc, wd, we, wf)
    fs = lax.axis_index("fs")
    t = lax.axis_index("tp")
    z = fs // PLANE
    p = fs % PLANE
    rows, width = tokens.shape
    half = rows // 2
    quarter = half // 2
    q, pw = w.shape[1], width // RING
    ds = wa.shape[1]
    qh = q // 2

    def dev(zz, pp, tt):
        return {"fs": zz * PLANE + pp, "tp": tt}

    peers = (p, p + 1 - 2 * (p % 2), (p + 2) % PLANE, PLANE - 1 - p)

    zc, zb, zo = (z + 1) % RING, (z + RING - 1) % RING, (z + 2) % RING
    cw, ccw, sibling = dev(zc, p, t), dev(zb, p, t), dev(z, p, 1 - t)
    to_peer = [dev(z, pp, t) for pp in peers]

    def remote(src, dst, s, r, to):
        return pltpu.make_async_remote_copy(
            src_ref=src, dst_ref=dst, send_sem=s, recv_sem=r,
            device_id=to, device_id_type=pl.DeviceIdType.MESH,
        )

    mine = pl.ds(pl.multiple_of(t * half, 16), half)
    other = pl.ds(pl.multiple_of((1 - t) * half, 16), half)

    barrier = pltpu.get_barrier_semaphore()
    targets = [cw, ccw, sibling] + to_peer[1:]
    for to in targets:
        pl.semaphore_signal(barrier, inc=1, device_id=to, device_id_type=pl.DeviceIdType.MESH)
    pl.semaphore_wait(barrier, len(targets))

    def p1_lanes(pp):
        return pl.ds(pl.multiple_of((z * PLANE + pp) * ds, ds), ds)

    def p1(m, r):
        src = shards_in[m].at[pl.ds(pl.multiple_of(peers[r] * q, 16), q), :]
        return remote(src, w.at[m, :, p1_lanes(p)], p1_s.at[m, r - 1], p1_r.at[m, r - 1], to_peer[r])

    def p1_local(m):
        src = shards_in[m].at[pl.ds(pl.multiple_of(p * q, 16), q), :]
        return pltpu.make_async_copy(src, w.at[m, :, p1_lanes(p)], p1_l.at[m])

    def p1_in(m, r):
        src = w.at[m, :, p1_lanes(peers[r])]
        return remote(src, src, p1_s.at[m, r - 1], p1_r.at[m, r - 1], to_peer[r])

    def start_p1(m):
        for r in (3, 1, 2):
            p1(m, r).start()
        p1_local(m).start()

    def blk(m, zz, lo=0, n=None):
        return w.at[m, pl.ds(lo, q if n is None else n), pl.ds(pl.multiple_of(zz * pw, pw), pw)]

    def ring(m, k, zz):
        return remote(blk(m, zz), blk(m, zz), ring_s.at[m, k], ring_r.at[m, k], (cw, ccw)[k])

    def fwd(m, k, zz):
        return remote(blk(m, zz, k * qh, qh), blk(m, zz, k * qh, qh), fwd_s.at[m, k], fwd_r.at[m, k], (cw, ccw)[k])

    def own_ring(m):
        p1_local(m).wait()
        for r in (1, 2, 3):
            p1_in(m, r).wait_recv()
        ring(m, 0, z).start()
        ring(m, 1, z).start()

    def service(m):
        ring(m, 0, zb).wait_recv()
        fwd(m, 0, zb).start()
        ring(m, 1, zc).wait_recv()
        fwd(m, 1, zc).start()

    def arrived(m):
        fwd(m, 0, zo).wait_recv()
        fwd(m, 1, zo).wait_recv()

    bufs = (normed1, normed2)

    def piece(tt, h):
        return pl.ds(pl.multiple_of(tt * half + h * quarter, 16), quarter)

    def ag(f, r, h):
        at = piece(t, h)
        return remote(bufs[f].at[0, at, :], bufs[f].at[r, at, :], ag_s.at[f, r - 1, h], ag_r.at[f, r - 1, h], to_peer[r])

    def ag_on(f, h):
        at = piece(t, h)
        return remote(bufs[f].at[2 - h, at, :], bufs[f].at[3, at, :], ag_s.at[f, 2, h], ag_r.at[f, 2, h], to_peer[1 + h])

    def relay(f, r, h, tt):
        at = bufs[f].at[r, piece(tt, h), :]
        return remote(at, at, rel_s.at[f, r, h], rel_r.at[f, r, h], sibling)

    def ag_near(f):
        for r, h in ((2, 0), (1, 1)):
            ag(f, r, h).wait_recv()
            ag_on(f, h).start()
            relay(f, r, h, t).start()
        for r, h in ((2, 1), (1, 0)):
            ag(f, r, h).wait_recv()
            relay(f, r, h, t).start()

    def ag_far(f):
        for h in range(2):
            ag_on(f, h).wait_recv()
            relay(f, 3, h, t).start()

    def relayed(f, r):
        for h in range(2):
            relay(f, r, h, 1 - t).wait_recv()

    lanes = [pl.ds(pl.multiple_of(zz * pw, pw), pw) for zz in (z, zb, zc, zo)]
    first, second = pl.ds(0, quarter), pl.ds(quarter, quarter)

    def to_sibling(f, c, r):
        return remote(part.at[r, :, lanes[c]], sib.at[r, :, lanes[c]], sib_s.at[f, c, r], sib_r.at[f, c, r], sibling)

    def rs(f, c, kind):
        at = lanes[c]
        src, dst, r = (
            (comb.at[2, first, at], diag.at[0, :, at], 1),
            (comb.at[2, second, at], diag.at[1, :, at], 2),
            (comb.at[0, first, at], rsr.at[0, first, at], 1),
            (comb.at[0, second, at], rsr.at[0, second, at], 1),
            (comb.at[1, second, at], rsr.at[1, second, at], 2),
            (comb.at[1, first, at], rsr.at[1, first, at], 2),
        )[kind]
        return remote(src, dst, rs_s.at[f, c, kind], rs_r.at[f, c, kind], to_peer[r])

    def make_hidden(f, slot):
        @pl.loop(0, 2)
        def _(i):
            at = pl.ds(pl.multiple_of(i * half, 16), half)
            x = bufs[f][slot, at, :]
            dims = (((1,), (1,)), ((), ()))
            g = lax.dot_general(x, w[3 * f], dims, preferred_element_type=F32)
            u = lax.dot_general(x, w[3 * f + 1], dims, preferred_element_type=F32)
            hidden[slot, at, :] = (g / (1.0 + jnp.exp(-g)) * u).astype(BF16)

    def make_down(f, c):
        at = lanes[c]

        @pl.loop(0, PLANE)
        def _(k):
            r = PLANE - 1 - k
            part[r, :, at] = jnp.dot(hidden[r, other, :], w[3 * f + 2, :, at], preferred_element_type=F32).astype(BF16)
            to_sibling(f, c, r).start()
            own[r, :, at] = jnp.dot(hidden[r, mine, :], w[3 * f + 2, :, at], preferred_element_type=F32).astype(BF16)

    step = 16

    def down(f, c):
        at = lanes[c]
        make_down(f, c)
        for r, kinds in ((3, (0, 1)), (1, (2,)), (2, (4,))):
            to_sibling(f, c, r).wait_recv()

            @pl.loop(0, half // (2 * step))
            def _(i):
                some = pl.ds(pl.multiple_of(i * 2 * step, step), 2 * step)
                comb[r - 1, some, at] = (own[r, some, at].astype(F32) + sib[r, some, at].astype(F32)).astype(BF16)

            for kind in kinds:
                rs(f, c, kind).start()
        to_sibling(f, c, 0).wait_recv()

    def finish(f, c):
        at = lanes[c]
        rs(f, c, 0).wait_recv()
        comb[1, first, at] = (comb[1, first, at].astype(F32) + diag[0, :, at].astype(F32)).astype(BF16)
        rs(f, c, 5).start()
        rs(f, c, 1).wait_recv()
        comb[0, second, at] = (comb[0, second, at].astype(F32) + diag[1, :, at].astype(F32)).astype(BF16)
        rs(f, c, 3).start()

    def all_down(f, before_last):
        down(f, 0)
        service(3 * f + 2)
        before_last()
        down(f, 1)
        finish(f, 0)
        down(f, 2)
        finish(f, 1)
        arrived(3 * f + 2)
        down(f, 3)
        finish(f, 2)
        finish(f, 3)

    def landed(f):
        for c in range(RING):
            for kind in (2, 3, 4, 5):
                rs(f, c, kind).wait_recv()

    def reduced(at):
        total = own[0, at, :].astype(F32) + sib[0, at, :].astype(F32)
        return total + rsr[0, at, :].astype(F32) + rsr[1, at, :].astype(F32)

    start_p1(0)
    start_p1(1)
    start_p1(2)

    @pl.loop(0, rows // step)
    def _(i):
        at = pl.ds(pl.multiple_of(i * step, step), step)
        normed1[0, at, :] = norm_rows(tokens[at, :].astype(F32), gain1[...]).astype(BF16)

    for r, h in ((2, 0), (1, 1), (2, 1), (1, 0)):
        ag(0, r, h).start()
    for m in (3, 4, 5):
        start_p1(m)
    own_ring(0)
    own_ring(1)
    service(0)
    own_ring(2)
    ag_near(0)
    service(1)
    own_ring(3)
    ag_far(0)
    arrived(0)
    arrived(1)
    for r in range(PLANE):
        if r:
            relayed(0, r)
        make_hidden(0, r)
    all_down(0, lambda: own_ring(4))
    service(3)
    own_ring(5)
    landed(0)
    for h in range(2):

        @pl.loop(0, quarter // step)
        def _(i):
            at = pl.ds(pl.multiple_of(h * quarter + i * step, step), step)
            full = pl.ds(pl.multiple_of(t * half + h * quarter + i * step, step), step)
            value = tokens[full, :].astype(F32) + merged[full, :].astype(F32) + 0.5 * reduced(at)
            middle[at, :] = value
            normed2[0, full, :] = norm_rows(value, gain2[...]).astype(BF16)

        for r in (2 - h, 1 + h):
            ag(1, r, h).start()
        relay(1, 0, h, t).start()

    ag_near(1)
    service(4)
    ag_far(1)
    arrived(3)
    arrived(4)
    for r in range(PLANE):
        relayed(1, r)
        make_hidden(1, r)
    for c in range(RING):
        for r in range(PLANE):
            to_sibling(0, c, r).wait_send()
        for kind in range(6):
            rs(0, c, kind).wait_send()
    all_down(1, lambda: None)
    landed(1)

    @pl.loop(0, half // step)
    def _(i):
        at = pl.ds(pl.multiple_of(i * step, step), step)
        full = pl.ds(pl.multiple_of(t * half + i * step, step), step)
        out[full, :] = (middle[at, :] + 0.5 * reduced(at)).astype(BF16)

    last = remote(out.at[mine, :], fin, fin_s, fin_r, sibling)
    last.start()
    for m in range(6):
        for r in (1, 2, 3):
            p1(m, r).wait_send()
        for k in range(2):
            ring(m, k, z).wait_send()
            fwd(m, k, (zb, zc)[k]).wait_send()
    for f in range(2):
        for h in range(2):
            for r in (1, 2):
                ag(f, r, h).wait_send()
            ag_on(f, h).wait_send()
            for r in range(1 - f, PLANE):
                relay(f, r, h, t).wait_send()
    for c in range(RING):
        for r in range(PLANE):
            to_sibling(1, c, r).wait_send()
        for kind in range(6):
            rs(1, c, kind).wait_send()
    last.wait_recv()
    out[other, :] = fin[...]
    last.wait_send()


def plane_shards(tokens, merged, gain1, g1, u1, d1, gain2, g2, u2, d2):
    rows, width = tokens.shape
    half = rows // 2
    q = d1.shape[0] // PLANE
    vmem = pl.BlockSpec(memory_space=pltpu.VMEM)
    dma = lambda *s: pltpu.SemaphoreType.DMA(s)
    return pl.pallas_call(
        kernel,
        out_shape=jax.ShapeDtypeStruct((rows, width), BF16),
        in_specs=[vmem] * 10,
        out_specs=vmem,
        scratch_shapes=[
            pltpu.VMEM((6, q, width), BF16),
            pltpu.VMEM((PLANE, rows, width), BF16),
            pltpu.VMEM((PLANE, rows, width), BF16),
            pltpu.VMEM((PLANE, rows, q), BF16),
            pltpu.VMEM((PLANE, half, width), BF16),
            pltpu.VMEM((PLANE, half, width), BF16),
            pltpu.VMEM((PLANE, half, width), BF16),
            pltpu.VMEM((PLANE - 1, half, width), BF16),
            pltpu.VMEM((2, half // 2, width), BF16),
            pltpu.VMEM((2, half, width), BF16),
            pltpu.VMEM((half, width), F32),
            pltpu.VMEM((half, width), BF16),
            dma(6, 3), dma(6, 3), dma(6),
            dma(6, 2), dma(6, 2), dma(6, 2), dma(6, 2),
            dma(2, 3, 2), dma(2, 3, 2), dma(2, 4, 2), dma(2, 4, 2),
            dma(2, RING, 4), dma(2, RING, 4), dma(2, RING, 6), dma(2, RING, 6),
            pltpu.SemaphoreType.DMA, pltpu.SemaphoreType.DMA,
        ],
        compiler_params=pltpu.CompilerParams(
            collective_id=0, has_side_effects=True, vmem_limit_bytes=60 * 2**20
        ),
    )(tokens, merged, gain1[None], gain2[None], g1.T, u1.T, d1, g2.T, u2.T, d2)


def shards(n_fs, n_tp, *args):
    rows, width = args[0].shape
    hid, cols = args[5].shape
    fits = n_fs == PLANE * RING and n_tp == 2 and cols % 128 == 0
    fits = fits and hid % (32 * PLANE) == 0 and rows % 64 == 0
    return plane_shards(*args) if fits else gathered_shards(*args)


def solution(mesh):
    return jax.shard_map(
        functools.partial(shards, mesh.shape["fs"], mesh.shape["tp"]),
        mesh=mesh,
        in_specs=(
            P("fs", None),
            P("fs", None),
            P(),
            P("fs", "tp"),
            P("fs", "tp"),
            P("tp", "fs"),
            P(),
            P("fs", "tp"),
            P("fs", "tp"),
            P("tp", "fs"),
        ),
        out_specs=P("fs", None),
        check_vma=False,
    )
```

time: 247 us -> 202 us (0.82); the launches traced: 243 us -> 202 us
  Pallas kernels: 234 us -> 194 us
    pallas_call x1, Pallas kernels: 234 us -> 194 us  [plane_shards(): pl.pallas_call(kernel, out_shape=jax.ShapeDtypeStruct((rows, width), BF16...]
where the time goes in v2:
time: 202 us
  Pallas kernels  194 us (96%)
  local copies, waits for them, and re-layouts  8.42 us (4%)
    pallas_call x1, Pallas kernels, plane_shards(): pl.pallas_call(kernel, out_shape=jax.ShapeDtypeStruct((rows, width), BF16...  194 us
    unnamed x9, local copies, waits for them, and re-layouts  8.42 us

profile of v2, /device:TPU:0, one launch (start us, length us, event | category | flops | bytes accessed | tf_op | source)
XLA Modules:
  0.0 202.1 jit_solution(6513895156052450390)
XLA Ops:
  0.0 0.0 copy-start.1
  0.0 0.0 copy-start
  0.0 2.0 copy.11
  2.0 1.9 copy.12
  3.8 0.0 copy-done
  3.9 0.9 copy.13
  4.8 0.0 copy-done.1
  4.8 0.9 copy.14
  5.7 193.6 %shard_map.100 = bf16[384,2048]{1,0:T(8,128)(2,1)} custom-call(bf16[384,2048]{1,0:T(8,128)(2,1)} %tokens.1, bf16[384,2048]{1,0:T(8,128)(2,1)} %merged.1, f32[1,2048]{1,0:T(1,128)} %bitcast.10, f32[1,2048]{1,0:T(1,128)} %bitcast.11, bf16[1408,128]{1,0:T(8,128)(2,1)} %bitcast.6, bf16[1408,128]{1,0:T(8,128)(2,1)} %bitcast.7, bf16[1408,128]{1,0:T(8,128)(2,1)} %wc.1, ...), custom_call_target="tpu_custom_call" | custom-call | tf_op jit(solution)/shard_map/pallas_call | solution.py:349
  199.3 2.7 %copy.16 = bf16[384,2048]{1,0:T(8,128)(2,1)} copy(bf16[384,2048]{1,0:T(8,128)(2,1)} %shard_map.100) | data formatting | bytes 3145728
Async XLA Ops:
  0.0 4.8 %copy-start.1 = (bf16[128,1408]{1,0:T(8,128)(2,1)S(1)}, bf16[128,1408]{1,0:T(8,128)(2,1)}, u32[]{:S(2)}) copy-start(bf16[128,1408]{1,0:T(8,128)(2,1)} %param.18) | copy-start | bytes 1081348
  0.0 3.8 %copy-start = (bf16[128,1408]{1,0:T(8,128)(2,1)S(1)}, bf16[128,1408]{1,0:T(8,128)(2,1)}, u32[]{:S(2)}) copy-start(bf16[128,1408]{1,0:T(8,128)(2,1)} %param.17) | copy-start | bytes 1081348
